TPU v7x, 32 devices: a whole 2x2x4 slice. The times are simulated.
32 devices in a mesh: ep: 4 (over y, x), tp: 8 (over z, core).
Axes of the slice: x: 2, y: 2, z: 4, core: 2. Of those that a mesh axis runs over, the one named last changes fastest.
Arguments:
- tokens: bfloat16 [896, 4096], P('ep', 'tp'), may hold values from -6 to 6
- picks: int32 [4, 4, 56], P('ep'), may hold values from 0 to 223, as said below
- pick_weights: float32 [4, 4, 56], P('ep'), may hold values from 0.1 to 1
- gate_weight: bfloat16 [4, 1280, 4096], P('ep', 'tp'), may hold values from -0.09375 to 0.09375
- up_weight: bfloat16 [4, 1280, 4096], P('ep', 'tp'), may hold values from -0.09375 to 0.09375
- down_weight: bfloat16 [4, 1280, 4096], P('ep', None, 'tp'), may hold values from -0.15625 to 0.15625
- dense_gate: bfloat16 [5120, 4096], P('tp'), may hold values from -0.09375 to 0.09375
- dense_up: bfloat16 [5120, 4096], P('tp'), may hold values from -0.09375 to 0.09375
- dense_down: bfloat16 [5120, 4096], P('tp'), may hold values from -0.078125 to 0.078125
- branch_gate: float32 [4096], P('tp'), may hold values from -6 to 6
Outputs:
- mixed: bfloat16 [896, 4096], P('ep', 'tp')
Inputs may be any that keep to these rules, and one draw needn't show every extreme that they name: For each block s and expert e, the 56 entries picks[s, e, :] are distinct rows of that block.
All inputs are finite; a program needn't handle non-finite values.
Results may differ from a plain program's by a relative error of at most 0.014.
Values may be sent and summed in bfloat16 or wider, within the bound.
A program may use at most 64 MiB of HBM per device.

v0:
```python
import functools

import jax
import jax.numpy as jnp
from jax import lax
from jax.experimental import pallas as pl
from jax.experimental.pallas import tpu as pltpu
from jax.sharding import PartitionSpec as P

MESH = pl.DeviceIdType.MESH
BF = jnp.bfloat16
F32 = jnp.float32
CORES = 2
G = 2
NT = (((1,), (1,)), ((), ()))
NN = (((1,), (0,)), ((), ()))
TN = (((0,), (0,)), ((), ()))


def mm(a, b, dims=NN):
    return lax.dot_general(a, b, dims, preferred_element_type=F32)


def silu(v):
    return v / (1.0 + jnp.exp(-v))


def kernel(
    n_ep, n_tp, pad,
    tok_hbm, pk_in, pw_in, weg_hbm, weu_hbm, wed_hbm, wg_hbm, wu_hbm, wd_hbm, bg,
    out_ref,
    x, wg, wu, wd, weg, weu, wed, acc_g, acc_u, oh, pk, ch, acc_eg, acc_eu,
    hx, acc_o, eo, back, hd, ps, pr, own, ru, rd, su, sd, acc_d,
    w_sem, ag_recv, ag_up, ag_dn, ag_pt, c_recv, c_send, cf_recv, cf_send,
    h_recv, h_send, hf_recv, hf_send, e_recv, e_send, p_recv, p_send,
    ru_recv, ru_send, rd_recv, rd_send,
):
    nz = n_tp // CORES
    rows, dl = x.shape[1], x.shape[2]
    rh = rows // G
    s = lax.axis_index("ep")
    t = lax.axis_index("tp")
    z = t // CORES
    c = t % CORES
    partner = CORES * z + (1 - c)

    loads = [
        pltpu.make_async_copy(src, dst, w_sem.at[i])
        for i, (src, dst) in enumerate(
            [(tok_hbm, x.at[t]), (wg_hbm, wg), (wu_hbm, wu), (weg_hbm, weg),
             (weu_hbm, weu), (wd_hbm, wd), (wed_hbm, wed)]
        )
    ]
    for cp in loads:
        cp.start()

    barrier = pltpu.get_barrier_semaphore()
    pl.semaphore_signal(barrier, inc=1, device_id={"tp": partner}, device_id_type=MESH)
    for k in range(1, nz):
        pl.semaphore_signal(
            barrier, inc=1, device_id={"tp": CORES * ((z + k) % nz) + c}, device_id_type=MESH
        )
    for k in range(1, n_ep):
        pl.semaphore_signal(barrier, inc=1, device_id={"ep": (s + k) % n_ep}, device_id_type=MESH)

    slots = pk_in.shape[2]
    spread = (
        lax.broadcasted_iota(jnp.int32, (pad, slots), 0)
        == lax.broadcasted_iota(jnp.int32, (pad, slots), 1)
    ).astype(F32).astype(BF)

    def match(e):
        ids = lax.broadcasted_iota(jnp.int32, (rows, slots), 0)
        return ids == pk_in[0, pl.ds(e, 1), :]

    for e in range(n_ep):
        hot = match(e).astype(F32).astype(BF)
        oh[e * pad:(e + 1) * pad, :] = mm(spread, hot, NT).astype(BF)
    acc_g[...] = jnp.zeros_like(acc_g)
    acc_u[...] = jnp.zeros_like(acc_u)
    acc_eg[...] = jnp.zeros_like(acc_eg)
    acc_eu[...] = jnp.zeros_like(acc_eu)
    acc_o[...] = jnp.zeros_like(acc_o)

    def remote(src, dst, ssem, rsem, **dev):
        return pltpu.make_async_remote_copy(
            src_ref=src, dst_ref=dst, send_sem=ssem, recv_sem=rsem,
            device_id=dev, device_id_type=MESH,
        )

    def part(g):
        return pl.ds(g * rh, rh)

    up_dev = jnp.minimum(t + CORES, n_tp - CORES + c)
    dn_dev = jnp.maximum(t - CORES, c)

    def ag_copy(zi, g, ssem, dev):
        j = CORES * zi + c
        ref = x.at[j, part(g), :]
        return remote(ref, ref, ssem.at[zi, g], ag_recv.at[j, g], tp=dev)

    def ag_wait(j, g):
        ref = x.at[j, part(g), :]
        remote(ref, ref, ag_pt.at[0, 0], ag_recv.at[j, g], tp=partner).wait_recv()

    def c_copy(zi, e, src_rows, dst_rows, sem_e, rsem_e):
        j = CORES * zi + c
        return remote(
            pk.at[zi, pl.ds(pl.multiple_of(src_rows, pad), pad), :],
            ch.at[j, pl.ds(pl.multiple_of(dst_rows, pad), pad), :],
            c_send.at[zi, sem_e], c_recv.at[zi, rsem_e], ep=e,
        )

    def cf_copy(zi, core):
        ref = ch.at[CORES * zi + core]
        return remote(ref, ref, cf_send.at[zi], cf_recv.at[zi], tp=partner)

    def cols(j):
        return pl.ds(pl.multiple_of(j * dl, dl), dl)

    near = jnp.minimum(z, nz - 1 - z)

    def order(m):
        both = z + (1 - 2 * (m % 2)) * ((m + 1) // 2)
        far = jnp.where(2 * z < nz - 1, z + m - near, z - m + near)
        return jnp.where(m <= 2 * near, both, far)

    loads[0].wait()
    pl.semaphore_wait(barrier, 1 + (nz - 1) + (n_ep - 1))

    def forward(zi):
        for g in range(G):
            @pl.when(zi != z)
            def _():
                ag_wait(CORES * zi + c, g)

            @pl.when((zi <= z) & (z < nz - 1))
            def _():
                ag_copy(zi, g, ag_up, up_dev).start()

            @pl.when((zi >= z) & (z > 0))
            def _():
                ag_copy(zi, g, ag_dn, dn_dev).start()

            ag_copy(zi, g, ag_pt, partner).start()

    forward(z)

    def dense_block(j):
        acc_g[...] += mm(x[j], wg[:, cols(j)], NT)
        acc_u[...] += mm(x[j], wu[:, cols(j)], NT)

    @pl.loop(0, nz)
    def _(m):
        zi = order(m)
        mine = CORES * zi + c
        pk[zi] = mm(oh[...], x[mine]).astype(BF)
        for k in range(1, n_ep):
            e = (s + k) % n_ep
            c_copy(zi, e, e * pad, s * pad, e, s).start()
        keep = pl.ds(pl.multiple_of(s * pad, pad), pad)
        ch[mine, keep, :] = pk[zi, keep, :]

        @pl.when(m == 0)
        def _():
            loads[1].wait()
            loads[2].wait()

        dense_block(mine)

        @pl.when(m < nz - 1)
        def _():
            forward(order(m + 1))

        other = CORES * zi + (1 - c)
        for g in range(G):
            ag_wait(other, g)
        dense_block(other)

    hd[...] = (silu(acc_g[...]) * acc_u[...]).astype(BF)
    loads[5].wait()

    def p_copy(zi):
        return remote(ps.at[zi], pr.at[zi], p_send.at[zi], p_recv.at[zi], tp=partner)

    @pl.loop(0, nz)
    def _(zi):
        ps[zi] = mm(hd[...], wd[:, cols(CORES * zi + (1 - c))]).astype(BF)
        p_copy(zi).start()

    @pl.loop(0, nz)
    def _(zi):
        own[zi] = mm(hd[...], wd[:, cols(CORES * zi + c)]).astype(BF)
        p_copy(zi).wait_recv()
        own[zi] = (own[zi].astype(F32) + pr[zi].astype(F32)).astype(BF)

    def rs_up(zu, g, src):
        return remote(src.at[zu, part(g), :], ru.at[zu, part(g), :],
                      ru_send.at[zu, g], ru_recv.at[zu, g], tp=up_dev)

    def rs_dn(zd, g, src):
        return remote(src.at[zd, part(g), :], rd.at[zd, part(g), :],
                      rd_send.at[zd, g], rd_recv.at[zd, g], tp=dn_dev)

    @pl.when(z == 0)
    def _():
        @pl.loop(0, nz - 1)
        def _(i):
            for g in range(G):
                rs_up(nz - 1 - i, g, own).start()

    @pl.when(z == nz - 1)
    def _():
        @pl.loop(0, nz - 1)
        def _(i):
            for g in range(G):
                rs_dn(i, g, own).start()

    loads[3].wait()
    loads[4].wait()

    @pl.loop(0, nz)
    def _(m):
        zi = order(m)
        for k in range(1, n_ep):
            e = (s + k) % n_ep
            c_copy(zi, e, e * pad, e * pad, e, e).wait_recv()
        cf_copy(zi, c).start()

        @pl.loop(0, CORES)
        def _(q):
            j = CORES * zi + (c + q) % CORES

            @pl.when(q > 0)
            def _():
                cf_copy(zi, 1 - c).wait_recv()

            acc_eg[...] += mm(weg[:, cols(j)], ch[j], NT)
            acc_eu[...] += mm(weu[:, cols(j)], ch[j], NT)

    hx[t] = (silu(acc_eg[...]) * acc_eu[...]).astype(BF)

    def h_copy(zo, src_z, sidx):
        ref = hx.at[CORES * src_z + c]
        return remote(ref, ref, h_send.at[sidx], h_recv.at[src_z], tp=CORES * zo + c)

    def hf_copy(zi, core):
        ref = hx.at[CORES * zi + core]
        return remote(ref, ref, hf_send.at[zi], hf_recv.at[zi], tp=partner)

    for k in range(1, nz):
        zo = (z + k) % nz
        h_copy(zo, z, zo).start()
    hf_copy(z, c).start()

    @pl.when((z > 0) & (z < nz - 1))
    def _():
        @pl.loop(0, nz - 1)
        def _(i):
            zu = nz - 1 - i
            zd = i
            for g in range(G):
                @pl.when(zu > z)
                def _():
                    rs_up(zu, g, su).wait_recv()
                    su[zu, part(g), :] = (
                        own[zu, part(g), :].astype(F32) + ru[zu, part(g), :].astype(F32)
                    ).astype(BF)
                    rs_up(zu, g, su).start()

                @pl.when(zd < z)
                def _():
                    rs_dn(zd, g, sd).wait_recv()
                    sd[zd, part(g), :] = (
                        own[zd, part(g), :].astype(F32) + rd[zd, part(g), :].astype(F32)
                    ).astype(BF)
                    rs_dn(zd, g, sd).start()

    loads[6].wait()

    @pl.loop(0, nz)
    def _(m):
        zi = order(m)
        @pl.when(zi != z)
        def _():
            h_copy((z + 1) % nz, zi, z).wait_recv()
            hf_copy(zi, c).start()

        @pl.loop(0, CORES)
        def _(q):
            j = CORES * zi + (c + q) % CORES

            @pl.when(q > 0)
            def _():
                hf_copy(zi, 1 - c).wait_recv()

            acc_o[...] += mm(hx[j], wed[j], TN)

    eo[...] = acc_o[...].astype(BF)

    def e_copy(dev, src_i, dst_i, ssem, rsem):
        return remote(
            eo.at[pl.ds(pl.multiple_of(src_i * pad, pad), pad), :],
            back.at[pl.ds(pl.multiple_of(dst_i * pad, pad), pad), :],
            e_send.at[ssem], e_recv.at[rsem], ep=dev,
        )

    for k in range(1, n_ep):
        e = (s + k) % n_ep
        e_copy(e, e, s, e, s).start()
    keep = pl.ds(pl.multiple_of(s * pad, pad), pad)
    back[keep, :] = eo[keep, :]

    acc_d[...] = own[z].astype(F32)

    @pl.when(z > 0)
    def _():
        for g in range(G):
            rs_up(z, g, su).wait_recv()
            acc_d[part(g), :] += ru[z, part(g), :].astype(F32)

    @pl.when(z < nz - 1)
    def _():
        for g in range(G):
            rs_dn(z, g, sd).wait_recv()
            acc_d[part(g), :] += rd[z, part(g), :].astype(F32)

    acc_d[...] = acc_d[...] * (1.0 / (1.0 + jnp.exp(-bg[...])))
    for k in range(1, n_ep):
        e = (s + k) % n_ep
        e_copy(e, e, e, e, e).wait_recv()
    for e in range(n_ep):
        sel = jnp.where(match(e), pw_in[0, pl.ds(e, 1), :], 0.0)
        hi = sel.astype(BF)
        lo = (sel - hi.astype(F32)).astype(BF)
        got = back[e * pad:(e + 1) * pad, :]
        acc_d[...] += mm(mm(hi, spread, NT).astype(BF), got) + mm(mm(lo, spread, NT).astype(BF), got)
    out_ref[...] = acc_d[...].astype(BF)

    @pl.loop(0, nz)
    def _(zi):
        for g in range(G):
            @pl.when((zi <= z) & (z < nz - 1))
            def _():
                ag_copy(zi, g, ag_up, up_dev).wait_send()

            @pl.when((zi >= z) & (z > 0))
            def _():
                ag_copy(zi, g, ag_dn, dn_dev).wait_send()

            ag_copy(zi, g, ag_pt, partner).wait_send()

            @pl.when(zi > z)
            def _():
                rs_up(zi, g, su).wait_send()

            @pl.when(zi < z)
            def _():
                rs_dn(zi, g, sd).wait_send()

        for k in range(1, n_ep):
            e = (s + k) % n_ep
            c_copy(zi, e, e * pad, s * pad, e, s).wait_send()
        cf_copy(zi, c).wait_send()
        p_copy(zi).wait_send()
        hf_copy(zi, c).wait_send()

        @pl.when(zi != z)
        def _():
            h_copy((z + 1) % nz, z, zi).wait_send()

    for k in range(1, n_ep):
        e = (s + k) % n_ep
        e_copy(e, e, s, e, s).wait_send()


def per_device(
    n_ep, n_tp, tokens, picks, pick_weights, gate_weight, up_weight, down_weight,
    dense_gate, dense_up, dense_down, branch_gate,
):
    rows, dl = tokens.shape
    slots = picks.shape[2]
    pad = -(-slots // 16) * 16
    nz = n_tp // CORES
    he, width = gate_weight.shape[1], gate_weight.shape[2]
    hd = dense_gate.shape[0]
    ep_rows = n_ep * pad
    vm = pl.BlockSpec(memory_space=pltpu.VMEM)
    hbm = pl.BlockSpec(memory_space=pl.ANY)
    sem = pltpu.SemaphoreType.DMA
    blocks = pltpu.VMEM((nz, rows, dl), BF)
    return pl.pallas_call(
        functools.partial(kernel, n_ep, n_tp, pad),
        out_shape=jax.ShapeDtypeStruct((rows, dl), BF),
        in_specs=[hbm, vm, vm, hbm, hbm, hbm, hbm, hbm, hbm, vm],
        out_specs=vm,
        scratch_shapes=[
            pltpu.VMEM((n_tp, rows, dl), BF),
            pltpu.VMEM((hd, width), BF),
            pltpu.VMEM((hd, width), BF),
            pltpu.VMEM((hd, width), BF),
            pltpu.VMEM((he, width), BF),
            pltpu.VMEM((he, width), BF),
            pltpu.VMEM((n_tp, he, dl), BF),
            pltpu.VMEM((rows, hd), F32),
            pltpu.VMEM((rows, hd), F32),
            pltpu.VMEM((ep_rows, rows), BF),
            pltpu.VMEM((nz, ep_rows, dl), BF),
            pltpu.VMEM((n_tp, ep_rows, dl), BF),
            pltpu.VMEM((he, ep_rows), F32),
            pltpu.VMEM((he, ep_rows), F32),
            pltpu.VMEM((n_tp, he, ep_rows), BF),
            pltpu.VMEM((ep_rows, dl), F32),
            pltpu.VMEM((ep_rows, dl), BF),
            pltpu.VMEM((ep_rows, dl), BF),
            pltpu.VMEM((rows, hd), BF),
            blocks, blocks, blocks, blocks, blocks, blocks, blocks,
            pltpu.VMEM((rows, dl), F32),
            sem((7,)),
            sem((n_tp, G)), sem((nz, G)), sem((nz, G)), sem((nz, G)),
            sem((nz, n_ep)), sem((nz, n_ep)), sem((nz,)), sem((nz,)),
            sem((nz,)), sem((nz,)), sem((nz,)), sem((nz,)),
            sem((n_ep,)), sem((n_ep,)), sem((nz,)), sem((nz,)),
            sem((nz, G)), sem((nz, G)), sem((nz, G)), sem((nz, G)),
        ],
        compiler_params=pltpu.CompilerParams(
            collective_id=0, has_side_effects=True, vmem_limit_bytes=60 * 1024 * 1024
        ),
    )(
        tokens, picks, pick_weights,
        gate_weight[0], up_weight[0], down_weight[0].reshape(n_tp, he, dl),
        dense_gate, dense_up, dense_down, branch_gate.reshape(1, -1),
    )


def solution(mesh):
    in_specs = (
        P("ep", "tp"),
        P("ep", None, None),
        P("ep", None, None),
        P("ep", "tp", None),
        P("ep", "tp", None),
        P("ep", None, "tp"),
        P("tp", None),
        P("tp", None),
        P("tp", None),
        P("tp"),
    )
    return jax.shard_map(
        functools.partial(per_device, mesh.shape["ep"], mesh.shape["tp"]),
        mesh=mesh, in_specs=in_specs, out_specs=P("ep", "tp"), check_vma=False,
    )
```

profile of v0, /device:TPU:8, one launch (start us, length us, event | category | flops | bytes accessed | tf_op | source)
XLA Modules:
  0.0 63.9 jit_solution(8899165737125490973)
XLA Ops:
  0.0 62.2 %shard_map.100 = bf16[224,512]{1,0:T(8,128)(2,1)} custom-call(bf16[224,512]{1,0:T(8,128)(2,1)} %tok_hbm.1, s32[1,4,56]{2,1,0:T(4,128)} %pk_in.1, f32[1,4,56]{2,1,0:T(4,128)} %pw_in.1, bf16[160,4096]{1,0:T(8,128)(2,1)} %bitcast.4, bf16[160,4096]{1,0:T(8,128)(2,1)} %bitcast.5, bf16[8,160,512]{2,1,0:T(8,128)(2,1)} %bitcast.6, bf16[640,4096]{1,0:T(8,128)(2,1)} %wg_hbm.1, ...), custom_call_target="tpu_custom_call" | custom-call | tf_op jit(solution)/shard_map/pallas_call | solution.py:392
  62.3 1.6 %copy.12 = bf16[224,512]{1,0:T(8,128)(2,1)} copy(bf16[224,512]{1,0:T(8,128)(2,1)} %shard_map.100) | data formatting | bytes 458752
where the time goes:
time: 64.4 us; the launch traced here: 63.9 us
  Pallas kernels  62.2 us (97%)
  local copies, waits for them, and re-layouts  1.64 us (3%)
    pallas_call x1, Pallas kernels, per_device(): pl.pallas_call(functools.partial(kernel, n_ep, n_tp, pad), out_shape=jax....  62.2 us
    unnamed x1, local copies, waits for them, and re-layouts  1.64 us

commit v1 on v0

v1 whole, which is shorter than its diff:
```python
import functools

import jax
import jax.numpy as jnp
from jax import lax
from jax.experimental import pallas as pl
from jax.experimental.pallas import tpu as pltpu
from jax.sharding import PartitionSpec as P

MESH = pl.DeviceIdType.MESH
BF = jnp.bfloat16
F32 = jnp.float32
CORES = 2
R = 2
NT = (((1,), (1,)), ((), ()))
NN = (((1,), (0,)), ((), ()))
TN = (((0,), (0,)), ((), ()))
scope = jax.named_scope


def mm(a, b, dims=NN):
    return lax.dot_general(a, b, dims, preferred_element_type=F32)


def silu(v):
    return v / (1.0 + jnp.exp(-v))


def kernel(
    n_ep, n_tp, pad, F,
    tok_hbm, pk_in, pw_in, weg_hbm, weu_hbm, wed_hbm, wg_hbm, wu_hbm, wd_hbm, bg,
    out_ref,
    x, w, wd, we, wed, acc, oh, whi, wlo, pk, ch, acc_e,
    hx, acc_o, eo, back, hd, ps, pr, own, ru, rd, su, sd, acc_d,
    w_sem, ag_recv, ag_up, ag_dn, ag_pt, c_recv, c_send, cf_recv, cf_send,
    h_recv, h_send, hf_recv, hf_send, e_recv, e_send, p_recv, p_send,
    ru_recv, ru_send, rd_recv, rd_send,
):
    nz = n_tp // CORES
    rows, df = x.shape[1], x.shape[2]
    dl = F * df
    rc = rows // R
    hdn = hd.shape[1]
    he = hx.shape[1]
    s = lax.axis_index("ep")
    t = lax.axis_index("tp")
    z = t // CORES
    c = t % CORES
    partner = CORES * z + (1 - c)
    low = 2 * z < nz - 1
    end = (z == 0) | (z == nz - 1)
    mid = (z > 0) & (z < nz - 1)

    def load(i, src, dst):
        return pltpu.make_async_copy(src, dst, w_sem.at[i])

    tok_loads = [
        load(6 + f, tok_hbm.at[:, pl.ds(f * df, df)], x.at[t * F + f]) for f in range(F)
    ]
    loads = [
        load(0, wg_hbm, w.at[pl.ds(0, hdn), :]),
        load(1, wu_hbm, w.at[pl.ds(hdn, hdn), :]),
        load(2, wd_hbm, wd),
        load(3, weg_hbm, we.at[pl.ds(0, he), :]),
        load(4, weu_hbm, we.at[pl.ds(he, he), :]),
        load(5, wed_hbm, wed),
    ]
    barrier = pltpu.get_barrier_semaphore()
    for cp in tok_loads:
        cp.start()
    pl.semaphore_signal(barrier, inc=1, device_id={"tp": partner}, device_id_type=MESH)

    @pl.when(z > 0)
    def _():
        pl.semaphore_signal(
            barrier, inc=1, device_id={"tp": jnp.maximum(t - CORES, c)}, device_id_type=MESH
        )

    @pl.when(z < nz - 1)
    def _():
        pl.semaphore_signal(
            barrier, inc=1, device_id={"tp": jnp.minimum(t + CORES, n_tp - CORES + c)},
            device_id_type=MESH,
        )

    for k in range(1, n_ep):
        pl.semaphore_signal(barrier, inc=1, device_id={"ep": (s + k) % n_ep}, device_id_type=MESH)
    for cp in loads:
        cp.start()

    def remote(src, dst, ssem, rsem, **dev):
        return pltpu.make_async_remote_copy(
            src_ref=src, dst_ref=dst, send_sem=ssem, recv_sem=rsem,
            device_id=dev, device_id_type=MESH,
        )

    def rws(r):
        return pl.ds(r * rc, rc)

    up_dev = jnp.minimum(t + CORES, n_tp - CORES + c)
    dn_dev = jnp.maximum(t - CORES, c)

    def ag_copy(zi, f, r, ssem, dev):
        b = (CORES * zi + c) * F + f
        ref = x.at[b, rws(r), :]
        return remote(ref, ref, ssem.at[zi * F + f, r], ag_recv.at[b, r], tp=dev)

    def ag_wait(j, f, r):
        b = j * F + f
        ref = x.at[b, rws(r), :]
        remote(ref, ref, ag_pt.at[0, 0], ag_recv.at[b, r], tp=partner).wait_recv()

    def c_copy(b, blk, e, src_rows, dst_rows, sem_e, rsem_e):
        return remote(
            pk.at[b, pl.ds(pl.multiple_of(src_rows, pad), pad), :],
            ch.at[blk, pl.ds(pl.multiple_of(dst_rows, pad), pad), :],
            c_send.at[b, sem_e], c_recv.at[b, rsem_e], ep=e,
        )

    def cf_copy(zi, f, core):
        ref = ch.at[(CORES * zi + core) * F + f]
        return remote(ref, ref, cf_send.at[zi * F + f], cf_recv.at[zi * F + f], tp=partner)

    def cols(b):
        return pl.ds(pl.multiple_of(b * df, df), df)

    def wide(j):
        return pl.ds(pl.multiple_of(j * dl, dl), dl)

    near = jnp.minimum(z, nz - 1 - z)

    def order(m):
        both = z + (1 - 2 * (m % 2)) * ((m + 1) // 2)
        far = jnp.where(2 * z < nz - 1, z + m - near, z - m + near)
        return jnp.where(m <= 2 * near, both, far)

    def send_on(zi, f, r):
        @pl.when((zi <= z) & (z < nz - 1))
        def _():
            ag_copy(zi, f, r, ag_up, up_dev).start()

        @pl.when((zi >= z) & (z > 0))
        def _():
            ag_copy(zi, f, r, ag_dn, dn_dev).start()

        ag_copy(zi, f, r, ag_pt, partner).start()

    def forward(zi, r):
        for f in range(F):
            ag_wait(CORES * zi + c, f, r)
            send_on(zi, f, r)

    with scope("tokwait"):
        for cp in tok_loads:
            cp.wait()
    with scope("barrier"):
        pl.semaphore_wait(
            barrier,
            n_ep + jnp.where(z > 0, 1, 0) + jnp.where(z < nz - 1, 1, 0),
        )
    for r in range(R):
        for f in range(F):
            send_on(z, f, r)

    slots = pk_in.shape[2]
    ep_rows = n_ep * pad
    spread = (
        lax.broadcasted_iota(jnp.int32, (pad, slots), 0)
        == lax.broadcasted_iota(jnp.int32, (pad, slots), 1)
    ).astype(F32).astype(BF)

    with scope("prep"):
        for e in range(n_ep):
            ids = lax.broadcasted_iota(jnp.int32, (rows, slots), 0)
            hit = ids == pk_in[0, pl.ds(e, 1), :]
            oh[e * pad:(e + 1) * pad, :] = mm(spread, hit.astype(F32).astype(BF), NT).astype(BF)
        place_hi = jnp.zeros((rows, ep_rows), F32)
        place_lo = jnp.zeros((rows, ep_rows), F32)
        for e in range(n_ep):
            ids = lax.broadcasted_iota(jnp.int32, (rows, slots), 0)
            sel = jnp.where(ids == pk_in[0, pl.ds(e, 1), :], pw_in[0, pl.ds(e, 1), :], 0.0)
            hi = sel.astype(BF)
            lo = (sel - hi.astype(F32)).astype(BF)
            at = (
                lax.broadcasted_iota(jnp.int32, (slots, ep_rows), 0) + e * pad
                == lax.broadcasted_iota(jnp.int32, (slots, ep_rows), 1)
            ).astype(F32).astype(BF)
            place_hi += mm(hi, at)
            place_lo += mm(lo, at)
        whi[...] = place_hi.astype(BF)
        wlo[...] = place_lo.astype(BF)
        acc[...] = jnp.zeros_like(acc)
        acc_e[...] = jnp.zeros_like(acc_e)
        acc_o[...] = jnp.zeros_like(acc_o)

    def dense_block(j, r):
        v = mm(x[j * F, rws(r), :], w[:, cols(j * F)], NT)
        for f in range(1, F):
            v += mm(x[j * F + f, rws(r), :], w[:, cols(j * F + f)], NT)
        acc[rws(r), :] += v

    def pick(zi):
        mine = (CORES * zi + c) * F
        for f in range(F):
            b = zi * F + f
            pk[b] = mm(oh[...], x[mine + f]).astype(BF)
            for k in range(1, n_ep):
                e = (s + n_ep - k) % n_ep
                c_copy(b, mine + f, e, e * pad, s * pad, e, s).start()
            keep = pl.ds(pl.multiple_of(s * pad, pad), pad)
            ch[mine + f, keep, :] = pk[b, keep, :]

    def dense_pair(zi, r):
        with scope("dmine"):
            dense_block(CORES * zi + c, r)
        other = CORES * zi + (1 - c)
        with scope("dwait"):
            for f in range(F):
                ag_wait(other, f, r)
        with scope("dother"):
            dense_block(other, r)

    def p_copy(zi, r):
        return remote(
            ps.at[zi, rws(r), :], pr.at[zi, rws(r), :],
            p_send.at[zi, r], p_recv.at[zi, r], tp=partner,
        )

    def rs_up(zu, f, r, src):
        b = zu * F + f
        return remote(src.at[b, rws(r), :], ru.at[b, rws(r), :],
                      ru_send.at[b, r], ru_recv.at[b, r], tp=up_dev)

    def rs_dn(zd, f, r, src):
        b = zd * F + f
        return remote(src.at[b, rws(r), :], rd.at[b, rws(r), :],
                      rd_send.at[b, r], rd_recv.at[b, r], tp=dn_dev)

    def partials(r):
        def far(i):
            return jnp.where(low, nz - 1 - i, i)

        with scope("ps"):
            @pl.loop(0, nz)
            def _(i):
                zi = far(i)
                ps[zi, rws(r), :] = mm(
                    hd[rws(r), :], wd[:, wide(CORES * zi + (1 - c))]
                ).astype(BF)
                p_copy(zi, r).start()

        with scope("own"):
            @pl.loop(0, nz)
            def _(i):
                zi = far(i)
                v = mm(hd[rws(r), :], wd[:, wide(CORES * zi + c)])
                p_copy(zi, r).wait_recv()
                v += pr[zi, rws(r), :].astype(F32)
                for f in range(F):
                    own[zi * F + f, rws(r), :] = v[:, f * df:(f + 1) * df].astype(BF)

                @pl.when((z == 0) & (zi > z))
                def _():
                    for f in range(F):
                        rs_up(zi, f, r, own).start()

                @pl.when((z == nz - 1) & (zi < z))
                def _():
                    for f in range(F):
                        rs_dn(zi, f, r, own).start()

    for r in range(R):
        last = r == R - 1

        @pl.loop(0, nz)
        def _(m):
            zi = order(m)

            @pl.when((m > 0) & ((jnp.abs(zi - z) > 1) | (r == 0)))
            def _():
                with scope(f"fwd{r}"):
                    forward(zi, r)

            if last:
                with scope("pick"):
                    pick(zi)
            if r == 0:
                @pl.when(m == 0)
                def _():
                    with scope("wload"):
                        loads[0].wait()
                        loads[1].wait()
            dense_pair(zi, r)

        if not last:
            with scope("fwdnear"):
                @pl.when(z > 0)
                def _():
                    forward(jnp.maximum(z - 1, 0), r + 1)

                @pl.when(z < nz - 1)
                def _():
                    forward(jnp.minimum(z + 1, nz - 1), r + 1)

        hid = acc[rws(r), :]
        hd[rws(r), :] = (silu(hid[:, :hdn]) * hid[:, hdn:]).astype(BF)
        if r == 0:
            loads[2].wait()
        if not last:
            @pl.when(end)
            def _():
                partials(r)
        else:
            @pl.when(mid)
            def _():
                for q in range(R - 1):
                    partials(q)

            partials(r)

    loads[3].wait()
    loads[4].wait()

    def emm(j):
        with scope("emm"):
            v = mm(we[:, cols(j * F)], ch[j * F], NT)
            for f in range(1, F):
                v += mm(we[:, cols(j * F + f)], ch[j * F + f], NT)
            acc_e[...] += v

    def emm_other(zi):
        with scope("cfwait"):
            for f in range(F):
                cf_copy(zi, f, 1 - c).wait_recv()
        emm(CORES * zi + (1 - c))

    @pl.loop(0, nz)
    def _(m):
        zi = order(m)
        mine = (CORES * zi + c) * F
        with scope("cwait"):
            for f in range(F):
                for k in range(1, n_ep):
                    e = (s + k) % n_ep
                    c_copy(zi * F + f, mine + f, e, e * pad, e * pad, e, e).wait_recv()
                cf_copy(zi, f, c).start()
        emm(CORES * zi + c)

        @pl.when(m > 0)
        def _():
            emm_other(order(jnp.maximum(m - 1, 0)))

    emm_other(order(nz - 1))
    he_acc = acc_e[...]
    hx[t] = (silu(he_acc[:he]) * he_acc[he:]).astype(BF)

    def h_copy(zo, src_z, sidx):
        ref = hx.at[CORES * src_z + c]
        return remote(ref, ref, h_send.at[sidx], h_recv.at[src_z], tp=CORES * zo + c)

    def hf_copy(zi, core):
        ref = hx.at[CORES * zi + core]
        return remote(ref, ref, hf_send.at[zi], hf_recv.at[zi], tp=partner)

    for k in range(1, nz):
        zo = (z + k) % nz
        h_copy(zo, z, zo).start()
    hf_copy(z, c).start()

    def turn(zu, f, r, hop, got, out, cond, name):
        @pl.when(cond)
        def _():
            with scope(name):
                b = zu * F + f
                hop(zu, f, r, out).wait_recv()
                out[b, rws(r), :] = (
                    own[b, rws(r), :].astype(F32) + got[b, rws(r), :].astype(F32)
                ).astype(BF)
                hop(zu, f, r, out).start()

    def ups(r, lo_i, hi_i):
        @pl.loop(lo_i, hi_i)
        def _(i):
            zu = nz - 1 - i
            for f in range(F):
                turn(zu, f, r, rs_up, ru, su, zu > z, f"up{r}")

    def dns(r, lo_i, hi_i):
        @pl.loop(lo_i, hi_i)
        def _(i):
            for f in range(F):
                turn(i, f, r, rs_dn, rd, sd, i < z, f"dn{r}")

    def relay(r, lo_i, hi_i, second):
        @pl.when(mid & low)
        def _():
            ups(r, lo_i, hi_i)
            if second:
                dns(r, 0, nz - 1)

        @pl.when(mid & jnp.logical_not(low))
        def _():
            dns(r, lo_i, hi_i)
            if second:
                ups(r, 0, nz - 1)

    for r in range(R - 1):
        relay(r, 0, nz - 1, True)
    relay(R - 1, 0, 1, False)

    loads[5].wait()

    def down(j):
        acc_o[...] += mm(hx[j], wed[j], TN)

    def down_other(zi):
        with scope("hfwait"):
            hf_copy(zi, 1 - c).wait_recv()
        with scope("down"):
            down(CORES * zi + (1 - c))

    @pl.loop(0, nz)
    def _(m):
        zi = order(m)

        @pl.when(zi != z)
        def _():
            with scope("hwait"):
                h_copy((z + 1) % nz, zi, z).wait_recv()
                hf_copy(zi, c).start()

        with scope("down"):
            down(CORES * zi + c)

        @pl.when(m > 0)
        def _():
            down_other(order(jnp.maximum(m - 1, 0)))

    down_other(order(nz - 1))
    eo[...] = acc_o[...].astype(BF)

    def e_copy(dev, src_i, dst_i, ssem, rsem):
        return remote(
            eo.at[pl.ds(pl.multiple_of(src_i * pad, pad), pad), :],
            back.at[pl.ds(pl.multiple_of(dst_i * pad, pad), pad), :],
            e_send.at[ssem], e_recv.at[rsem], ep=dev,
        )

    for k in range(1, n_ep):
        e = (s + n_ep - k) % n_ep
        e_copy(e, e, s, e, s).start()
    keep = pl.ds(pl.multiple_of(s * pad, pad), pad)
    back[keep, :] = eo[keep, :]

    relay(R - 1, 1, nz - 1, True)

    for f in range(F):
        acc_d[:, f * df:(f + 1) * df] = own[z * F + f].astype(F32)

    def finish(hop, got):
        for r in range(R):
            for f in range(F):
                hop(z, f, r, su).wait_recv()
                acc_d[rws(r), f * df:(f + 1) * df] += got[z * F + f, rws(r), :].astype(F32)

    @pl.when(z > 0)
    def _():
        with scope("finup"):
            finish(rs_up, ru)

    @pl.when(z < nz - 1)
    def _():
        with scope("findn"):
            finish(rs_dn, rd)

    acc_d[...] = acc_d[...] * (1.0 / (1.0 + jnp.exp(-bg[...])))

    with scope("sends"):
        @pl.loop(0, nz)
        def _(zi):
            for f in range(F):
                b = zi * F + f
                for r in range(R):
                    @pl.when((zi <= z) & (z < nz - 1))
                    def _():
                        ag_copy(zi, f, r, ag_up, up_dev).wait_send()

                    @pl.when((zi >= z) & (z > 0))
                    def _():
                        ag_copy(zi, f, r, ag_dn, dn_dev).wait_send()

                    ag_copy(zi, f, r, ag_pt, partner).wait_send()

                    @pl.when((zi > z) & (z < nz - 1))
                    def _():
                        rs_up(zi, f, r, su).wait_send()

                    @pl.when((zi < z) & (z > 0))
                    def _():
                        rs_dn(zi, f, r, sd).wait_send()

                for k in range(1, n_ep):
                    e = (s + k) % n_ep
                    c_copy(b, (CORES * zi + c) * F + f, e, e * pad, s * pad, e, s).wait_send()
                cf_copy(zi, f, c).wait_send()
            for r in range(R):
                p_copy(zi, r).wait_send()
            hf_copy(zi, c).wait_send()

            @pl.when(zi != z)
            def _():
                h_copy((z + 1) % nz, z, zi).wait_send()

    with scope("ewait"):
        for k in range(1, n_ep):
            e = (s + k) % n_ep
            e_copy(e, e, e, e, e).wait_recv()
    with scope("combine"):
        out_ref[...] = (
            acc_d[...] + (mm(whi[...], back[...]) + mm(wlo[...], back[...]))
        ).astype(BF)

    for k in range(1, n_ep):
        e = (s + k) % n_ep
        e_copy(e, e, s, e, s).wait_send()


def per_device(
    n_ep, n_tp, tokens, picks, pick_weights, gate_weight, up_weight, down_weight,
    dense_gate, dense_up, dense_down, branch_gate,
):
    rows, dl = tokens.shape
    slots = picks.shape[2]
    pad = -(-slots // 16) * 16
    nz = n_tp // CORES
    he, width = gate_weight.shape[1], gate_weight.shape[2]
    hd = dense_gate.shape[0]
    ep_rows = n_ep * pad
    F = 2 if dl % 256 == 0 else 1
    df = dl // F
    vm = pl.BlockSpec(memory_space=pltpu.VMEM)
    hbm = pl.BlockSpec(memory_space=pl.ANY)
    sem = pltpu.SemaphoreType.DMA
    parts = pltpu.VMEM((nz * F, rows, df), BF)
    return pl.pallas_call(
        functools.partial(kernel, n_ep, n_tp, pad, F),
        out_shape=jax.ShapeDtypeStruct((rows, dl), BF),
        in_specs=[hbm, vm, vm, hbm, hbm, hbm, hbm, hbm, hbm, vm],
        out_specs=vm,
        scratch_shapes=[
            pltpu.VMEM((n_tp * F, rows, df), BF),
            pltpu.VMEM((2 * hd, width), BF),
            pltpu.VMEM((hd, width), BF),
            pltpu.VMEM((2 * he, width), BF),
            pltpu.VMEM((n_tp, he, dl), BF),
            pltpu.VMEM((rows, 2 * hd), F32),
            pltpu.VMEM((ep_rows, rows), BF),
            pltpu.VMEM((rows, ep_rows), BF),
            pltpu.VMEM((rows, ep_rows), BF),
            pltpu.VMEM((nz * F, ep_rows, df), BF),
            pltpu.VMEM((n_tp * F, ep_rows, df), BF),
            pltpu.VMEM((2 * he, ep_rows), F32),
            pltpu.VMEM((n_tp, he, ep_rows), BF),
            pltpu.VMEM((ep_rows, dl), F32),
            pltpu.VMEM((ep_rows, dl), BF),
            pltpu.VMEM((ep_rows, dl), BF),
            pltpu.VMEM((rows, hd), BF),
            pltpu.VMEM((nz, rows, dl), BF),
            pltpu.VMEM((nz, rows, dl), BF),
            parts, parts, parts, parts, parts,
            pltpu.VMEM((rows, dl), F32),
            sem((6 + F,)),
            sem((n_tp * F, R)), sem((nz * F, R)), sem((nz * F, R)), sem((nz * F, R)),
            sem((nz * F, n_ep)), sem((nz * F, n_ep)), sem((nz * F,)), sem((nz * F,)),
            sem((nz,)), sem((nz,)), sem((nz,)), sem((nz,)),
            sem((n_ep,)), sem((n_ep,)), sem((nz, R)), sem((nz, R)),
            sem((nz * F, R)), sem((nz * F, R)), sem((nz * F, R)), sem((nz * F, R)),
        ],
        compiler_params=pltpu.CompilerParams(
            collective_id=0, has_side_effects=True, vmem_limit_bytes=60 * 1024 * 1024
        ),
    )(
        tokens, picks, pick_weights,
        gate_weight[0], up_weight[0], down_weight[0].reshape(n_tp, he, dl),
        dense_gate, dense_up, dense_down, branch_gate.reshape(1, -1),
    )


def solution(mesh):
    in_specs = (
        P("ep", "tp"),
        P("ep", None, None),
        P("ep", None, None),
        P("ep", "tp", None),
        P("ep", "tp", None),
        P("ep", None, "tp"),
        P("tp", None),
        P("tp", None),
        P("tp", None),
        P("tp"),
    )
    return jax.shard_map(
        functools.partial(per_device, mesh.shape["ep"], mesh.shape["tp"]),
        mesh=mesh, in_specs=in_specs, out_specs=P("ep", "tp"), check_vma=False,
    )
```

time: 64.4 us -> 58.8 us (0.913)
  the two profiles are of different devices: /device:TPU:8 before, /device:TPU:0 now
where the time goes in v1:
time: 58.8 us; the launch traced here: 58.6 us
  Pallas kernels  57 us (97%)
  local copies, waits for them, and re-layouts  1.64 us (3%)
    pallas_call x1, Pallas kernels, per_device(): pl.pallas_call(functools.partial(kernel, n_ep, n_tp, pad, F), out_shape=j...  57 us
    unnamed x1, local copies, waits for them, and re-layouts  1.64 us

profile of v1, /device:TPU:0, one launch (start us, length us, event | category | flops | bytes accessed | tf_op | source)
XLA Modules:
  0.0 58.6 jit_solution(4549722284279387830)
XLA Ops:
  0.0 57.0 %shard_map.100 = bf16[224,512]{1,0:T(8,128)(2,1)} custom-call(bf16[224,512]{1,0:T(8,128)(2,1)} %tok_hbm.1, s32[1,4,56]{2,1,0:T(4,128)} %pk_in.1, f32[1,4,56]{2,1,0:T(4,128)} %pw_in.1, bf16[160,4096]{1,0:T(8,128)(2,1)} %bitcast.4, bf16[160,4096]{1,0:T(8,128)(2,1)} %bitcast.5, bf16[8,160,512]{2,1,0:T(8,128)(2,1)} %bitcast.6, bf16[640,4096]{1,0:T(8,128)(2,1)} %wg_hbm.1, ...), custom_call_target="tpu_custom_call" | custom-call | tf_op jit(solution)/shard_map/pallas_call | solution.py:545
  57.0 1.6 %copy.12 = bf16[224,512]{1,0:T(8,128)(2,1)} copy(bf16[224,512]{1,0:T(8,128)(2,1)} %shard_map.100) | data formatting | bytes 458752
